TPU v7x, 512 devices: a whole 4x8x8 slice. The times are simulated.
512 devices in a mesh: sp: 64 (over z, y), tp: 8 (over x, core).
Axes of the slice: x: 4, y: 8, z: 8, core: 2. Of those that a mesh axis runs over, the one named last changes fastest.
Arguments:
- target: bfloat16 [16384, 2048], P(('sp', 'tp')), may hold values from -6 to 6
- source: bfloat16 [16384, 2048], P(('sp', 'tp')), may hold values from -6 to 6
- target_gain: float32 [2, 2048], replicated, may hold values from 0.1 to 1.9
- source_gain: float32 [2, 2048], replicated, may hold values from 0.1 to 1.9
- query_gain: float32 [2, 64], replicated, may hold values from 0.75 to 2.75
- key_gain: float32 [2, 64], replicated, may hold values from 0.75 to 2.75
- query_weight: bfloat16 [2, 2048, 512], P(None, None, 'tp'), may hold values from -0.125 to 0.125
- key_weight: bfloat16 [2, 2048, 128], replicated, may hold values from -0.125 to 0.125
- value_weight: bfloat16 [2, 2048, 128], replicated, may hold values from -0.125 to 0.125
- out_weight: bfloat16 [2, 512, 2048], P(None, 'tp'), may hold values from -0.25 to 0.25
Outputs:
- decoded: bfloat16 [16384, 2048], P(('sp', 'tp'))
All inputs are finite; a program needn't handle non-finite values.
Results may differ from a plain program's by a relative error of at most 0.014.
Values may be sent and summed in bfloat16 or wider, within the bound.
No kernel may reach another device: no remote copies, remote signals or barrier semaphores. Data moves between devices by JAX's collectives and lax.ppermute only.
A program may use at most 64 MiB of HBM per device.

v0:
```python
import jax
import jax.numpy as jnp
from jax import lax
from jax.sharding import Mesh
from jax.sharding import PartitionSpec as P

SP = ("sp_0", "sp_1")
SP_TP = ("sp_0", "sp_1", "tp")


epsilon = 1e-06


def sent_to_all(value, axis):
    copies = jnp.broadcast_to(value, (lax.axis_size(axis), *value.shape))
    return lax.all_to_all(copies, axis, split_axis=0, concat_axis=0, tiled=True)


def joined_along(tiles, dim):
    dims = list(tiles.shape[1:])
    dims[dim] *= tiles.shape[0]
    return jnp.moveaxis(tiles, 0, dim).reshape(dims)


def gather_directly(value, axis, dim):
    tiles = sent_to_all(value, axis)
    return joined_along(tiles, dim)


def gather_in_order(value, axes, sequence):
    tiles = value
    for k in sequence:
        tiles = lax.all_gather(tiles, axes[k])
    done = sequence[::-1]
    back = [done.index(k) for k in range(len(axes))]
    tiles = tiles.transpose(*back, *range(len(axes), tiles.ndim))
    return tiles.reshape(-1, *value.shape)


def gathered_by_axis(value, axes, sequence, dim):
    return joined_along(gather_in_order(value, axes, sequence), dim)


def in_blocks(value, dim, devices):
    before, after = (value.shape[:dim], value.shape[dim + 1 :])
    return jnp.moveaxis(value.reshape(*before, devices, -1, *after), dim, 0)


def sent_and_summed(value, axis, dim):
    tiles = in_blocks(value, dim, lax.axis_size(axis))
    arrived = lax.all_to_all(tiles, axis, split_axis=0, concat_axis=0, tiled=True)
    return arrived.astype(jnp.float32).sum(axis=0)


def row_norm(values, gain_row):
    inverse = lax.rsqrt(jnp.mean(values * values, axis=-1, keepdims=True) + epsilon)
    return values * inverse * gain_row


def partial_softmax(queries, key_rows, value_rows):
    score_scale = queries.shape[-1] ** (-0.5)
    scores = (
        jnp.einsum("qd,kd->qk", queries, key_rows, preferred_element_type=jnp.float32) * score_scale
    )
    weights = jnp.exp(scores)
    weighted = jnp.dot(weights.astype(jnp.bfloat16), value_rows, preferred_element_type=jnp.float32)
    return (weighted, jnp.sum(weights, axis=1))


def fold_keys(queries, head_size, shard_rows, running, kv_piece):

    def absorb_block(partial_value, one_block):
        weighted, total_mass = partial_softmax(
            queries, one_block[:, :head_size], one_block[:, head_size:]
        )
        return ((partial_value[0] + weighted, partial_value[1] + total_mass), None)

    piece_rows = kv_piece.shape[0]
    shards = piece_rows // shard_rows
    factor = max(
        [
            divisor
            for divisor in range(1, shards + 1)
            if shards % divisor == 0 and divisor * shard_rows <= 2048
        ]
    )
    block_rows = factor * shard_rows
    blocks = kv_piece.reshape(piece_rows // block_rows, block_rows, kv_piece.shape[1])
    result, unused = lax.scan(absorb_block, running, blocks)
    return result


def body(
    target,
    source,
    target_gain,
    source_gain,
    query_gain,
    key_gain,
    query_weight,
    key_weight,
    value_weight,
    out_weight,
):
    tp_size = lax.axis_size("tp")
    layers = query_weight.shape[0]
    head_size = query_gain.shape[1]
    key_heads = key_weight.shape[2] // head_size
    local_heads = query_weight.shape[2] // head_size
    source_rows = source.shape[0]
    source_float = source.astype(jnp.float32)
    source_scale = lax.rsqrt(
        jnp.mean(source_float * source_float, axis=-1, keepdims=True) + epsilon
    )
    stacked = []
    for layer_index in range(layers):
        normed = (source_float * source_scale * source_gain[layer_index]).astype(jnp.bfloat16)
        keys_now = jnp.dot(normed, key_weight[layer_index], preferred_element_type=jnp.float32)
        keys_now = row_norm(
            keys_now.reshape(source_rows, key_heads, head_size), key_gain[layer_index]
        ).astype(jnp.bfloat16)
        values_now = jnp.dot(
            normed, value_weight[layer_index], preferred_element_type=jnp.float32
        ).astype(jnp.bfloat16)
        values_now = values_now.reshape(source_rows, key_heads, head_size)
        stacked.append(jnp.concatenate([keys_now, values_now], axis=2))
    packed = jnp.stack(stacked, axis=2).reshape(source_rows, key_heads, layers * 2 * head_size)
    outgoing = jnp.repeat(packed, tp_size // key_heads, axis=1)
    arrived = lax.all_to_all(outgoing, "tp", split_axis=1, concat_axis=0, tiled=True)
    arrived = arrived.reshape(-1, layers, 2 * head_size)
    shard_rows = arrived.shape[0]
    hidden = target
    for layer_index in range(layers):
        hidden_float = hidden.astype(jnp.float32)
        normed = row_norm(hidden_float, target_gain[layer_index]).astype(jnp.bfloat16)
        weight_now = query_weight[layer_index]
        projected = jnp.dot(
            gather_directly(normed, "tp", 0), weight_now, preferred_element_type=jnp.float32
        )
        group_rows = projected.shape[0]
        queries = row_norm(
            projected.reshape(group_rows, local_heads, head_size), query_gain[layer_index]
        ).astype(jnp.bfloat16)
        query_count = group_rows * local_heads
        queries = queries.reshape(query_count, head_size)
        pair_rows = arrived[:, layer_index, :]
        starting = (
            jnp.zeros((query_count, head_size), jnp.float32),
            jnp.zeros((query_count,), jnp.float32),
        )
        weighted, total_mass = fold_keys(
            queries, head_size, shard_rows, starting, gathered_by_axis(pair_rows, SP, (0, 1), 0)
        )
        attended = (weighted / total_mass[:, None]).astype(jnp.bfloat16)
        out_now = out_weight[layer_index]
        mixed_rows = sent_and_summed(
            jnp.dot(attended, out_now, preferred_element_type=jnp.float32).astype(jnp.bfloat16),
            "tp",
            0,
        )
        hidden = (hidden_float + mixed_rows).astype(jnp.bfloat16)
    return hidden


def solution(mesh):
    split = Mesh(mesh.devices.reshape(8, 8, mesh.shape["tp"]), ("sp_0", "sp_1", "tp"))
    return jax.shard_map(
        body,
        mesh=split,
        in_specs=(
            P(SP_TP, None),
            P(SP_TP, None),
            P(),
            P(),
            P(),
            P(),
            P(None, None, "tp"),
            P(),
            P(),
            P(None, "tp", None),
        ),
        out_specs=P(SP_TP, None),
        check_vma=False,
    )
```

profile of v0, /device:TPU:1, one launch (start us, length us, event | category | flops | bytes accessed | tf_op | source)
XLA Modules:
  0.0 221.5 jit_solution(10086685425758472452)
XLA Ops:
  6.5 1.1 fusion.16
  7.7 0.8 fusion.50
  8.5 1.4 slice_bitcast_fusion.1
  12.3 14.5 %all_to_all.35 = bf16[32,8,256]{2,0,1:T(8,128)(2,1)S(1)} all-to-all(bf16[32,8,256]{2,0,1:T(8,128)(2,1)S(1)} %bitcast.121), channel_id=1, replica_groups=mesh['sp_0'=8,'sp_1'=8,'tp'=8] {'tp'}, dimensions={1} | all-to-all | bytes 262144 | tf_op jit(solution)/shard_map/all_to_all | solution.py:129
  27.0 24.3 %all-gather = bf16[2048,1,128]{2,0,1:T(8,128)(2,1)} all-gather(bf16[256,1,128]{2,0,1:T(8,128)(2,1)S(1)} %copy.36), channel_id=2, replica_groups=mesh['sp_0'=8,'sp_1'=8,'tp'=8] {'sp_0'}, dimensions={0}, use_global_device_ids=true | all-gather | bytes 589824 | tf_op jit(solution)/shard_map/all_gather | solution.py:33
  51.6 1.2 broadcast_in_dim.7
  52.8 10.2 %all-to-all-start.1 = ((bf16[8,32,2048]{2,1,0:T(8,128)(2,1)}), bf16[8,32,2048]{2,1,0:T(8,128)(2,1)S(1)}, u32[]{:S(2)}, u32[]{:S(2)}) async-start(bf16[8,32,2048]{2,1,0:T(8,128)(2,1)} %broadcast_in_dim.7), calls=%async_computation.1 | async-start | bytes 2097152 | tf_op jit(solution)/shard_map/all_to_all | solution.py:16
  63.0 23.1 %all-gather.2 = bf16[2048,1,128]{2,0,1:T(8,128)(2,1)} all-gather(bf16[256,1,128]{2,0,1:T(8,128)(2,1)S(1)} %copy.39), channel_id=4, replica_groups=mesh['sp_0'=8,'sp_1'=8,'tp'=8] {'sp_0'}, dimensions={0}, use_global_device_ids=true | all-gather | bytes 589824 | tf_op jit(solution)/shard_map/all_gather | solution.py:33
  86.8 24.0 %all-gather.7.cloned.1.call-done = bf16[64,256,128]{2,1,0:T(8,128)(2,1)} async-done(((bf16[8,256,128]{2,1,0:T(8,128)(2,1)}), bf16[64,256,128]{2,1,0:T(8,128)(2,1)}) %all-gather.7.cloned.1.call-update) | async-done | bytes 4194320 | tf_op jit(solution)/shard_map/all_gather | solution.py:33
  110.8 4.6 %copy.37 = bf16[8,8,256,128]{3,2,1,0:T(8,128)(2,1)} copy(bf16[8,8,256,128]{3,2,0,1:T(8,128)(2,1)} %bitcast.112) | data formatting | bytes 8388608 | tf_op jit(solution)/shard_map/transpose | solution.py:36
  115.4 18.8 %while.26 = (s32[]{:T(128)}, f32[256,64]{0,1:T(8,128)S(1)}, f32[256]{0:T(256)S(1)}, bf16[8,2048,128]{2,1,0:T(8,128)(2,1)}, bf16[256,64]{1,0:T(8,128)(2,1)S(1)}, /*index=5*/s32[]{:T(128)}, s32[]{:T(128)}) while((s32[]{:T(128)}, f32[256,64]{0,1:T(8,128)S(1)}, f32[256]{0:T(256)S(1)}, bf16[8,2048,128]{2,1,0:T(8,128)(2,1)}, ...), condition=%wide.region_7.8_spmd.clone, body=%wide.region_5.7_spmd.clone.sunk | while | flops 135823616 | bytes 4362332 | solution.py:89
  115.4 1.1 dynamic-slice_bitcast_fusion.4
  117.2 0.6 convolution_add_fusion.4
  117.8 1.1 dynamic-slice_bitcast_fusion.4
  119.5 0.6 convolution_add_fusion.4
  120.2 1.1 dynamic-slice_bitcast_fusion.4
  121.9 0.6 convolution_add_fusion.4
  122.5 1.1 dynamic-slice_bitcast_fusion.4
  124.2 0.6 convolution_add_fusion.4
  124.9 1.1 dynamic-slice_bitcast_fusion.4
  126.5 0.6 convolution_add_fusion.4
  127.2 1.1 dynamic-slice_bitcast_fusion.4
  128.9 0.6 convolution_add_fusion.4
  129.5 1.1 dynamic-slice_bitcast_fusion.4
  131.2 0.6 convolution_add_fusion.4
  131.9 1.1 dynamic-slice_bitcast_fusion.4
  133.6 0.6 convolution_add_fusion.4
  134.7 19.9 %all_to_all.36 = bf16[8,32,2048]{2,1,0:T(8,128)(2,1)S(1)} all-to-all(bf16[8,32,2048]{2,1,0:T(8,128)(2,1)S(1)} %bitcast.115), channel_id=1, replica_groups=mesh['sp_0'=8,'sp_1'=8,'tp'=8] {'tp'}, dimensions={0} | all-to-all | bytes 2097152 | tf_op jit(solution)/shard_map/all_to_all | solution.py:51
  155.0 1.2 broadcast_in_dim.8
  156.2 4.4 %all-to-all-start.3 = ((bf16[8,32,2048]{2,1,0:T(8,128)(2,1)}), bf16[8,32,2048]{2,1,0:T(8,128)(2,1)S(1)}, u32[]{:S(2)}, u32[]{:S(2)}) async-start(bf16[8,32,2048]{2,1,0:T(8,128)(2,1)} %broadcast_in_dim.8), calls=%async_computation.3 | async-start | bytes 2097152 | tf_op jit(solution)/shard_map/all_to_all | solution.py:16
  160.6 8.4 %all-gather.9.cloned.1.call-done = bf16[64,256,128]{2,1,0:T(8,128)(2,1)} async-done(((bf16[8,256,128]{2,1,0:T(8,128)(2,1)}), bf16[64,256,128]{2,1,0:T(8,128)(2,1)}) %all-gather.9.cloned.1.call-update) | async-done | bytes 4194320 | tf_op jit(solution)/shard_map/all_gather | solution.py:33
  169.0 4.6 %copy.40 = bf16[8,8,256,128]{3,2,1,0:T(8,128)(2,1)} copy(bf16[8,8,256,128]{3,2,0,1:T(8,128)(2,1)} %bitcast.111) | data formatting | bytes 8388608 | tf_op jit(solution)/shard_map/transpose | solution.py:36
  173.7 1.9 all-to-all-done.3
  176.3 18.7 %while.27 = (s32[]{:T(128)}, f32[256,64]{0,1:T(8,128)S(1)}, f32[256]{0:T(256)S(1)}, bf16[8,2048,128]{2,1,0:T(8,128)(2,1)}, bf16[256,64]{1,0:T(8,128)(2,1)S(1)}, /*index=5*/s32[]{:T(128)}, s32[]{:T(128)}) while((s32[]{:T(128)}, f32[256,64]{0,1:T(8,128)S(1)}, f32[256]{0:T(256)S(1)}, bf16[8,2048,128]{2,1,0:T(8,128)(2,1)}, ...), condition=%wide.region_13.14_spmd.clone, body=%wide.region_11.13_spmd.clone.sunk | while | flops 135823616 | bytes 4362332 | solution.py:89
  176.3 1.1 dynamic-slice_bitcast_fusion.5
  178.0 0.6 convolution_add_fusion.5
  178.6 1.1 dynamic-slice_bitcast_fusion.5
  180.3 0.6 convolution_add_fusion.5
  181.0 1.1 dynamic-slice_bitcast_fusion.5
  183.3 1.1 dynamic-slice_bitcast_fusion.5
  185.0 0.6 convolution_add_fusion.5
  185.7 1.1 dynamic-slice_bitcast_fusion.5
  188.0 1.1 dynamic-slice_bitcast_fusion.5
  190.3 1.1 dynamic-slice_bitcast_fusion.5
  192.0 0.6 convolution_add_fusion.5
  192.7 1.1 dynamic-slice_bitcast_fusion.5
  195.5 18.3 %all_to_all.37 = bf16[8,32,2048]{2,1,0:T(8,128)(2,1)S(1)} all-to-all(bf16[8,32,2048]{2,1,0:T(8,128)(2,1)S(1)} %bitcast.116), channel_id=1, replica_groups=mesh['sp_0'=8,'sp_1'=8,'tp'=8] {'tp'}, dimensions={0} | all-to-all | bytes 2097152 | tf_op jit(solution)/shard_map/all_to_all | solution.py:51
  213.9 0.7 fusion.24
  (104 shorter events, 17.9 us)
Async XLA Ops:
  6.5 3.5 %copy-start.1 = (bf16[32,2048]{1,0:T(8,128)(2,1)S(1)}, bf16[32,2048]{1,0:T(8,128)(2,1)}, u32[]{:S(2)}) copy-start(bf16[32,2048]{1,0:T(8,128)(2,1)} %param.15) | copy-start | bytes 393220
  6.5 104.3 %all-gather.7.cloned.1.call-start = ((), (), s32[]{:S(2)}) async-start(), calls=%async_computation.5 | async-start | bytes 4718592 | tf_op jit(solution)/shard_map/all_gather | solution.py:33
  8.5 2.3 %copy-start.7 = (bf16[2,2048,128]{2,1,0:T(8,128)(2,1)S(1)}, bf16[2,2048,128]{2,1,0:T(8,128)(2,1)}, u32[]{:S(2)}) copy-start(bf16[2,2048,128]{2,1,0:T(8,128)(2,1)} %param.22) | copy-start | bytes 3145732
  10.1 1.8 copy-start.5
  11.1 40.3 %copy-start = (bf16[32,2048]{1,0:T(8,128)(2,1)S(1)}, bf16[32,2048]{1,0:T(8,128)(2,1)}, u32[]{:S(2)}) copy-start(bf16[32,2048]{1,0:T(8,128)(2,1)} %param.14) | copy-start | bytes 393220
  11.1 40.4 %copy-start.4 = (f32[2,2048]{1,0:T(2,128)S(1)}, f32[2,2048]{1,0:T(2,128)}, u32[]{:S(2)}) copy-start(f32[2,2048]{1,0:T(2,128)} %param.16) | copy-start | bytes 49156
  51.3 11.7 %copy-start.6 = (f32[2,64]{1,0:T(2,128)S(1)}, f32[2,64]{1,0:T(2,128)}, u32[]{:S(2)}) copy-start(f32[2,64]{1,0:T(2,128)} %param.18) | copy-start | bytes 1540
  51.6 34.5 %copy-start.2 = (bf16[2,2048,64]{1,2,0:T(8,128)(2,1)S(1)}, bf16[2,2048,64]{1,2,0:T(8,128)(2,1)}, u32[]{:S(2)}) copy-start(bf16[2,2048,64]{1,2,0:T(8,128)(2,1)} %param.20) | copy-start | bytes 1572868
  52.8 33.3 %all-to-all-start.1 = ((bf16[8,32,2048]{2,1,0:T(8,128)(2,1)}), bf16[8,32,2048]{2,1,0:T(8,128)(2,1)S(1)}, u32[]{:S(2)}, u32[]{:S(2)}) async-start(bf16[8,32,2048]{2,1,0:T(8,128)(2,1)} %broadcast_in_dim.7), calls=%async_computation.1 | async-start | bytes 2097152 | tf_op jit(solution)/shard_map/all_to_all | solution.py:16
  63.0 106.0 %all-gather.9.cloned.1.call-start = ((), (), s32[]{:S(2)}) async-start(), calls=%async_computation.6 | async-start | bytes 4718592 | tf_op jit(solution)/shard_map/all_gather | solution.py:33
  115.4 18.8 %copy-start.3 = (bf16[2,64,2048]{2,1,0:T(8,128)(2,1)S(1)}, bf16[2,64,2048]{2,1,0:T(8,128)(2,1)}, u32[]{:S(2)}) copy-start(bf16[2,64,2048]{2,1,0:T(8,128)(2,1)} %param.23) | copy-start | bytes 1572868
  156.2 19.4 %all-to-all-start.3 = ((bf16[8,32,2048]{2,1,0:T(8,128)(2,1)}), bf16[8,32,2048]{2,1,0:T(8,128)(2,1)S(1)}, u32[]{:S(2)}, u32[]{:S(2)}) async-start(bf16[8,32,2048]{2,1,0:T(8,128)(2,1)} %broadcast_in_dim.8), calls=%async_computation.3 | async-start | bytes 2097152 | tf_op jit(solution)/shard_map/all_to_all | solution.py:16
Sparse Core Ops, SparseCore 0:
  51.5 59.2 all-gather.6
  112.9 56.0 all-gather.8
where the time goes:
time: 223 us; the launch traced here: 221 us
  blocking collectives  100 us (45%)
  waiting for transfers between devices  34.4 us (15%)
  local copies, waits for them, and re-layouts  32.3 us (14%)
  matrix products  22.7 us (10%)
  starting transfers between devices  14.6 us (7%)
  between operations  13.7 us (6%)
  other arithmetic  3.22 us (1%)
    all_gather x2, blocking collectives, gather_in_order(): tiles = lax.all_gather(tiles, axes[k])  47.3 us
    all_to_all x2, blocking collectives, sent_and_summed(): lax.all_to_all(tiles, axis, split_axis=0, concat_axis=0, tiled=True)  38.2 us
    all_gather x2, waiting for transfers between devices, gather_in_order(): tiles = lax.all_gather(tiles, axes[k])  32.4 us
    squeeze x16, local copies, waits for them, and re-layouts, fold_keys(): result, unused = lax.scan(absorb_block, running, blocks)  17.3 us
    all_to_all x2, starting transfers between devices, sent_to_all(): return lax.all_to_all(copies, axis, split_axis=0, concat_axis=0, tiled=True)  14.6 us
    all_to_all x1, blocking collectives, body(): lax.all_to_all(outgoing, 'tp', split_axis=1, concat_axis=0, tiled=True)  14.5 us
    dot_general x16, matrix products, partial_softmax(): jnp.dot(weights.astype(jnp.bfloat16), value_rows, preferred_element_type=...  9.9 us
    dot_general x16, matrix products, partial_softmax(): jnp.einsum('qd,kd->qk', queries, key_rows, preferred_element_type=jnp.flo...  9.5 us
  transfers between devices with their start and end apart: 4, of which 3 were waited for; matrix products, arithmetic and copies ran while one was open for 14% of the time, Pallas kernels for 0%

commit v1 on v0

v1 whole, which is shorter than its diff:
```python
import functools

import jax
import jax.numpy as jnp
from jax import lax
from jax.experimental import pallas as pl
from jax.experimental.pallas import tpu as pltpu
from jax.sharding import Mesh
from jax.sharding import PartitionSpec as P

ROWS = ("z", "y")
TP = ("x", "c")
ALL = ("z", "y", "x", "c")
EPS = 1e-06
LOG2E = 1.4426950408889634
F32 = jnp.float32
BF16 = jnp.bfloat16


def dot(a, b):
    return jnp.dot(a, b, preferred_element_type=F32)


def dot_t(a, b):
    return lax.dot_general(a, b, (((1,), (1,)), ((), ())), preferred_element_type=F32)


def rms(value):
    return lax.rsqrt(jnp.mean(value * value, axis=-1, keepdims=True) + EPS)


def head_norm(value, gain_row, head):
    rows, width = value.shape
    low = lax.broadcasted_iota(jnp.int32, (rows, 2 * head), 1) < head
    groups = []
    for start in range(0, width, 2 * head):
        part = value[:, start : start + 2 * head]
        square = part * part
        first = jnp.sum(jnp.where(low, square, 0.0), axis=-1, keepdims=True)
        second = jnp.sum(jnp.where(low, 0.0, square), axis=-1, keepdims=True)
        scale = lax.rsqrt(jnp.where(low, first, second) / head + EPS)
        groups.append(part * scale * gain_row)
    return groups


def doubled(row):
    return jnp.concatenate([row, row], axis=-1)


def source_kernel(source, gain, key_gain, key_weight, value_weight, out):
    layers, head = key_gain.shape
    value = source[...].astype(F32)
    scaled = value * rms(value)
    width = key_weight.shape[2]
    for layer in range(layers):
        normed = (scaled * gain[layer : layer + 1, :]).astype(BF16)
        keys = dot(normed, key_weight[layer])
        row = doubled(key_gain[layer : layer + 1, :])
        groups = head_norm(keys, row, head)
        for k, group in enumerate(groups):
            out[layer, :, k * 2 * head : (k + 1) * 2 * head] = group.astype(BF16)
        out[layer, :, width:] = dot(normed, value_weight[layer]).astype(BF16)


def project(normed, mine, other, row, head, core):
    own = head_norm(dot_t(normed, mine), row, head)
    far = head_norm(dot_t(normed, other), row, head)
    first = [jnp.where(core == 0, a, b) for a, b in zip(own, far)]
    second = [jnp.where(core == 0, b, a) for a, b in zip(own, far)]
    return first + second


def store_groups(out, groups, width):
    for k, group in enumerate(groups):
        out[:, k * width : (k + 1) * width] = group.astype(BF16)


def query_kernel(layer, core_ref, target, gain, query_gain, mine, other, out):
    head = query_gain.shape[1]
    value = target[...].astype(F32)
    normed = (value * rms(value) * gain[layer : layer + 1, :]).astype(BF16)
    row = doubled(query_gain[layer : layer + 1, :])
    store_groups(out, project(normed, mine[...], other[...], row, head, core_ref[0]), 2 * head)


def attended_halves(arrived, heads, head):
    total = arrived[0].astype(F32)
    for k in range(1, arrived.shape[0]):
        total = total + arrived[k].astype(F32)
    rows = total.shape[0]
    width = heads * head
    mass = total[:, width : width + heads] + total[:, width + heads : width + 2 * heads]
    low = lax.broadcasted_iota(jnp.int32, (rows, 2 * head), 1) < head
    groups = []
    for g in range(heads // 2):
        below = jnp.where(low, mass[:, 2 * g : 2 * g + 1], mass[:, 2 * g + 1 : 2 * g + 2])
        groups.append((total[:, 2 * g * head : 2 * (g + 1) * head] / below).astype(BF16))
    half = len(groups) // 2
    return jnp.concatenate(groups[:half], axis=1), jnp.concatenate(groups[half:], axis=1)


def mixed(core, arrived, hidden, mine, other, heads, head):
    even, odd = attended_halves(arrived, heads, head)
    own = jnp.where(core == 0, even, odd)
    far = jnp.where(core == 0, odd, even)
    branch = dot(own, mine[...]) + dot(far, other[...])
    return (hidden[...].astype(F32) + branch).astype(BF16)


def middle_kernel(layer, heads, core_ref, arrived, hidden, gain, query_gain, out_mine, out_other, mine, other, hidden_out, out):
    head = query_gain.shape[1]
    core = core_ref[0]
    now = mixed(core, arrived, hidden, out_mine, out_other, heads, head)
    hidden_out[...] = now
    value = now.astype(F32)
    normed = (value * rms(value) * gain[layer : layer + 1, :]).astype(BF16)
    row = doubled(query_gain[layer : layer + 1, :])
    store_groups(out, project(normed, mine[...], other[...], row, head, core), 2 * head)


def last_kernel(heads, head, core_ref, arrived, hidden, out_mine, out_other, hidden_out):
    hidden_out[...] = mixed(core_ref[0], arrived, hidden, out_mine, out_other, heads, head)


def attention_kernel(heads, head, tile, queries, pairs, out, rhs, value_t, gathered):
    keys = pairs.shape[0]
    width = 2 * head
    columns = queries.shape[0]
    factor = LOG2E * head**-0.5
    turned = jnp.transpose(queries[...].astype(F32)).astype(BF16)
    zero = jnp.zeros((head, columns), BF16)
    per = heads // 4
    for p in range(heads):
        kv = (p % 4) // 2
        rhs[p, kv * head : (kv + 1) * head, :] = turned[p * head : (p + 1) * head, :]
        rhs[p, (1 - kv) * head : (2 - kv) * head, :] = zero
    value_t[...] = jnp.transpose(pairs[:, width:].astype(F32)).astype(BF16)
    for kv in range(2):

        def one_head(j, carry, kv=kv):
            p = (j // 2) * 4 + 2 * kv + j % 2
            right = rhs[p]
            mass = jnp.zeros((8, columns), F32)
            total = None
            for t in range(keys // tile):
                score = dot(pairs[t * tile : (t + 1) * tile, :width], right)
                weight = jnp.exp2(score * factor)
                mass = mass + jnp.sum(weight.reshape(tile // 8, 8, columns), axis=0)
                part = dot(value_t[:, t * tile : (t + 1) * tile], weight.astype(BF16))
                total = part if total is None else total + part
            gathered[pl.ds(pl.multiple_of(p * head, head), head), :] = total[kv * head : (kv + 1) * head, :]
            mass = jnp.sum(mass, axis=0, keepdims=True)
            top = mass.astype(BF16).astype(F32)
            gathered[pl.ds(heads * head + p, 1), :] = top
            gathered[pl.ds(heads * head + heads + p, 1), :] = mass - top
            return carry

        lax.fori_loop(0, 2 * per, one_head, 0)
    rest = heads * head + 2 * heads
    gathered[rest:, :] = jnp.zeros((gathered.shape[0] - rest, columns), F32)
    out[...] = jnp.transpose(gathered[...]).astype(BF16)


def call(kernel, shapes, scratch=(), flops=1000000, prefetch=0):
    one = not isinstance(shapes, (list, tuple))
    specs = pl.BlockSpec(memory_space=pltpu.VMEM)
    return pl.pallas_call(
        kernel,
        out_shape=shapes,
        out_specs=specs if one else [specs] * len(shapes),
        scratch_shapes=list(scratch),
        compiler_params=pltpu.CompilerParams(vmem_limit_bytes=40 * 1024 * 1024),
        cost_estimate=pl.CostEstimate(flops=flops, bytes_accessed=1000000, transcendentals=0),
    )


def with_core(kernel, shapes, count, flops):
    one = not isinstance(shapes, (list, tuple))
    spec = pl.BlockSpec(memory_space=pltpu.VMEM)
    return pl.pallas_call(
        kernel,
        out_shape=shapes,
        in_specs=[pl.BlockSpec(memory_space=pltpu.SMEM)] + [spec] * count,
        out_specs=spec if one else [spec] * len(shapes),
        compiler_params=pltpu.CompilerParams(vmem_limit_bytes=40 * 1024 * 1024),
        cost_estimate=pl.CostEstimate(flops=flops, bytes_accessed=1000000, transcendentals=0),
    )


def to_all(value, axis):
    copies = jnp.broadcast_to(value, (lax.axis_size(axis), *value.shape))
    return lax.all_to_all(copies, axis, split_axis=0, concat_axis=0, tiled=True)


def body(target, source, target_gain, source_gain, query_gain, key_gain, query_weight, key_weight, value_weight, out_weight):
    layers, _, head_columns = query_weight.shape
    head = query_gain.shape[1]
    heads = head_columns // head * lax.axis_size(TP)
    rows, model = target.shape
    group = rows * lax.axis_size(TP)
    shapes = jax.ShapeDtypeStruct
    core = lax.axis_index("c").reshape(1)

    query_t = jnp.swapaxes(query_weight, 1, 2)

    def full(piece):
        mine = to_all(piece, "x").reshape(-1, model)
        other = lax.ppermute(mine, "c", [(0, 1), (1, 0)])
        return mine, other

    pairs = call(source_kernel, shapes((layers, rows, 2 * key_weight.shape[2]), BF16), flops=200000000)(
        source, source_gain, key_gain, key_weight, value_weight
    )
    query_full = [full(query_t[0])]
    arrived_pairs = [to_all(pairs[0], ROWS)]
    out_full = [full(out_weight[0])]
    query_full.append(full(query_t[1]))
    arrived_pairs.append(to_all(pairs[1], ROWS))
    out_full.append(full(out_weight[1]))

    width = heads * head
    wide = width + 128
    queries = with_core(functools.partial(query_kernel, 0), shapes((rows, width), BF16), 5, 200000000)(
        core, target, target_gain, query_gain, *query_full[0]
    )
    hidden = target
    for layer in range(layers):
        everyone = to_all(queries, TP).reshape(group, width)
        kv = arrived_pairs[layer].reshape(-1, 4 * head)
        partial = call(
            functools.partial(attention_kernel, heads, head, 256),
            shapes((group, wide), BF16),
            scratch=[
                pltpu.VMEM((heads, 2 * head, group), BF16),
                pltpu.VMEM((2 * head, kv.shape[0]), BF16),
                pltpu.VMEM((wide, group), F32),
            ],
            flops=5000000000,
        )(everyone, kv)
        arrived = lax.all_to_all(partial.reshape(-1, rows, wide), TP, split_axis=0, concat_axis=0, tiled=True)
        if layer + 1 < layers:
            hidden, queries = with_core(
                functools.partial(middle_kernel, layer + 1, heads),
                [shapes((rows, model), BF16), shapes((rows, width), BF16)],
                8,
                400000000,
            )(core, arrived, hidden, target_gain, query_gain, *out_full[layer], *query_full[layer + 1])
        else:
            hidden = with_core(functools.partial(last_kernel, heads, head), shapes((rows, model), BF16), 4, 200000000)(
                core, arrived, hidden, *out_full[layer]
            )
    return hidden


def solution(mesh):
    columns = mesh.shape["tp"]
    split = Mesh(mesh.devices.reshape(8, 8, columns // 2, 2), ALL)
    return jax.shard_map(
        body,
        mesh=split,
        in_specs=(P(ALL, None), P(ALL, None), P(), P(), P(), P(), P(None, None, TP), P(), P(), P(None, TP, None)),
        out_specs=P(ALL, None),
        check_vma=False,
    )
```

time: 223 us -> 215 us (0.964)
  starting transfers between devices: 14.6 us -> 63.5 us
  blocking collectives: 100 us -> 51.5 us
  waiting for transfers between devices: 34.4 us -> 61.7 us
  Pallas kernels: 0 us -> 24.3 us
  matrix products: 22.7 us -> 0 us
  local copies, waits for them, and re-layouts: 32.3 us -> 12.2 us
  between operations: 13.7 us -> 0.23 us
  other arithmetic: 3.22 us -> 0 us
    all_to_all x2 -> x6, waiting for transfers between devices: 1.94 us -> 59.1 us  [the longest x5 52 us: to_all(): return lax.all_to_all(copies, axis, split_axis=0, concat_axis=0, tiled=True)]
    all_gather x2 -> x0, blocking collectives: 47.3 us -> none  [gather_in_order(): tiles = lax.all_gather(tiles, axes[k])]
    all_to_all x2 -> x6, starting transfers between devices: 14.6 us -> 50.2 us  [the longest x5 45.7 us: to_all(): return lax.all_to_all(copies, axis, split_axis=0, concat_axis=0, tiled=True)]
    all_gather x2 -> x0, waiting for transfers between devices: 32.4 us -> none  [gather_in_order(): tiles = lax.all_gather(tiles, axes[k])]
    pallas_call x0 -> x6, Pallas kernels: none -> 24.3 us  [the longest x2 17.8 us: body(): call(functools.partial(attention_kernel, heads, head, 256), shapes((group...]
    dot_general x40 -> x0, matrix products: 22.7 us -> none  [the longest x16 9.9 us: partial_softmax(): jnp.dot(weights.astype(jnp.bfloat16), value_rows, preferred_element_type=...]
    squeeze x16 -> x3, local copies, waits for them, and re-layouts: 17.3 us -> 1.81 us  [the longest x1 1.07 us: body(): query_full.append(full(query_t[1]))]
    ppermute x0 -> x4, starting transfers between devices: none -> 13.3 us  [full(): other = lax.ppermute(mine, 'c', [(0, 1), (1, 0)])]
  transfers between devices with their start and end apart: 4 -> 10, of which waited for: 3 -> 8; matrix products, arithmetic and copies ran while one was open for 14% -> 0% of each run, Pallas kernels for 0% -> 10%
where the time goes in v1:
time: 215 us; the launch traced here: 213 us
  starting transfers between devices  63.5 us (30%)
  waiting for transfers between devices  61.7 us (29%)
  blocking collectives  51.5 us (24%)
  Pallas kernels  24.3 us (11%)
  local copies, waits for them, and re-layouts  12.2 us (6%)
    all_to_all x5, waiting for transfers between devices, to_all(): return lax.all_to_all(copies, axis, split_axis=0, concat_axis=0, tiled=True)  52 us
    all_to_all x5, starting transfers between devices, to_all(): return lax.all_to_all(copies, axis, split_axis=0, concat_axis=0, tiled=True)  45.7 us
    all_to_all x3, blocking collectives, to_all(): return lax.all_to_all(copies, axis, split_axis=0, concat_axis=0, tiled=True)  38.8 us
    pallas_call x2, Pallas kernels, body(): call(functools.partial(attention_kernel, heads, head, 256), shapes((group...  17.8 us
    ppermute x4, starting transfers between devices, full(): other = lax.ppermute(mine, 'c', [(0, 1), (1, 0)])  13.3 us
    all_to_all x1, blocking collectives, body(): lax.all_to_all(partial.reshape(-1, rows, wide), TP, split_axis=0, concat_...  12.7 us
    all_to_all x1, waiting for transfers between devices, body(): lax.all_to_all(partial.reshape(-1, rows, wide), TP, split_axis=0, concat_...  7.11 us
    broadcast_in_dim x8, local copies, waits for them, and re-layouts, to_all(): copies = jnp.broadcast_to(value, (lax.axis_size(axis), *value.shape))  5.63 us
  transfers between devices with their start and end apart: 10, of which 8 were waited for; matrix products, arithmetic and copies ran while one was open for 0% of the time, Pallas kernels for 10%

profile of v1, /device:TPU:1, one launch (start us, length us, event | category | flops | bytes accessed | tf_op | source)
XLA Modules:
  0.0 213.4 jit_solution(12864581296426296057)
XLA Ops:
  0.0 1.1 slice_bitcast_fusion
  1.1 1.1 broadcast_in_dim.24
  2.2 5.0 %all-to-all-start = ((bf16[4,64,2048]{2,1,0:T(8,128)(2,1)}), bf16[4,64,2048]{2,1,0:T(8,128)(2,1)S(1)}, u32[]{:S(2)}, u32[]{:S(2)}) async-start(bf16[4,64,2048]{2,1,0:T(8,128)(2,1)} %broadcast_in_dim.24), calls=%async_computation | async-start | bytes 2097152 | tf_op jit(solution)/shard_map/all_to_all | solution.py:192
  7.1 0.7 slice_bitcast_fusion.2
  7.9 9.0 %all-to-all-done = bf16[4,64,2048]{2,1,0:T(8,128)(2,1)S(1)} async-done(((bf16[4,64,2048]{2,1,0:T(8,128)(2,1)}), bf16[4,64,2048]{2,1,0:T(8,128)(2,1)S(1)}, u32[]{:S(2)}, u32[]{:S(2)}) %all-to-all-start) | async-done | bytes 1048608 | tf_op jit(solution)/shard_map/all_to_all | solution.py:192
  16.9 0.1 broadcast_in_dim.27
  17.0 12.2 %all_to_all.50 = bf16[4,64,2048]{2,1,0:T(8,128)(2,1)S(1)} all-to-all(bf16[4,64,2048]{2,1,0:T(8,128)(2,1)S(1)} %broadcast_in_dim.27), channel_id=1, replica_groups=mesh['z'=8,'y'=8,'x'=4,'c'=2] {'x'}, dimensions={0} | all-to-all | bytes 2097152 | tf_op jit(solution)/shard_map/all_to_all | solution.py:192
  29.2 1.1 broadcast_in_dim.28
  30.3 3.6 %all-to-all-start.5 = ((bf16[4,64,2048]{2,1,0:T(8,128)(2,1)}), bf16[4,64,2048]{2,1,0:T(8,128)(2,1)S(1)}, u32[]{:S(2)}, u32[]{:S(2)}) async-start(bf16[4,64,2048]{2,1,0:T(8,128)(2,1)} %broadcast_in_dim.28), calls=%async_computation.5 | async-start | bytes 2097152 | tf_op jit(solution)/shard_map/all_to_all | solution.py:192
  33.9 0.0 copy-done.5
  33.9 0.0 copy-done.9
  33.9 0.0 copy-start
  34.0 1.2 copy-done
  35.2 1.2 copy-done.1
  36.4 0.5 shard_map.101
  36.9 6.7 %all-to-all-done.5 = bf16[4,64,2048]{2,1,0:T(8,128)(2,1)S(1)} async-done(((bf16[4,64,2048]{2,1,0:T(8,128)(2,1)}), bf16[4,64,2048]{2,1,0:T(8,128)(2,1)S(1)}, u32[]{:S(2)}, u32[]{:S(2)}) %all-to-all-start.5) | async-done | bytes 1048608 | tf_op jit(solution)/shard_map/all_to_all | solution.py:192
  43.6 1.1 broadcast_in_dim.26
  44.7 27.3 %all-to-all-start.2 = ((bf16[64,32,256]{2,1,0:T(8,128)(2,1)}), bf16[64,32,256]{2,1,0:T(8,128)(2,1)}, u32[]{:S(2)}, u32[]{:S(2)}) async-start(bf16[64,32,256]{2,1,0:T(8,128)(2,1)} %broadcast_in_dim.26), calls=%async_computation.2 | async-start | bytes 2097152 | tf_op jit(solution)/shard_map/all_to_all | solution.py:192
  72.1 6.0 %collective-permute-start = (bf16[256,2048]{1,0:T(8,128)(2,1)S(1)}, bf16[256,2048]{1,0:T(8,128)(2,1)}, u32[]{:S(2)}, u32[]{:S(2)}) collective-permute-start(bf16[256,2048]{1,0:T(8,128)(2,1)S(1)} %bitcast.24), channel_id=1, source_target_pairs={{0,1},{1,0},{2,3},{3,2},{4,5},{5,4},{6,7},{7,6},{8,9},{9,8},{10,11... | collective-permute-start | bytes 3145736 | tf_op jit(solution)/shard_map/ppermute | solution.py:208
  78.1 0.0 copy-start.10
  78.1 2.4 %collective-permute-done.other = bf16[256,2048]{1,0:T(8,128)(2,1)} collective-permute-done((bf16[256,2048]{1,0:T(8,128)(2,1)S(1)}, bf16[256,2048]{1,0:T(8,128)(2,1)}, u32[]{:S(2)}, u32[]{:S(2)}) %collective-permute-start) | collective-permute-done | bytes 1048608 | tf_op jit(solution)/shard_map/ppermute | solution.py:208
  80.5 2.1 shard_map.100
  82.6 14.7 %all-to-all-done.2 = bf16[64,32,256]{2,1,0:T(8,128)(2,1)} async-done(((bf16[64,32,256]{2,1,0:T(8,128)(2,1)}), bf16[64,32,256]{2,1,0:T(8,128)(2,1)}, u32[]{:S(2)}, u32[]{:S(2)}) %all-to-all-start.2) | async-done | bytes 1048608 | tf_op jit(solution)/shard_map/all_to_all | solution.py:192
  97.3 14.5 %all_to_all.51 = bf16[8,32,512]{2,1,0:T(8,128)(2,1)S(1)} all-to-all(bf16[8,32,512]{2,1,0:T(8,128)(2,1)S(1)} %broadcast_in_dim.25), channel_id=1, replica_groups=mesh['z'=8,'y'=8,'x'=4,'c'=2] {'x','c'}, dimensions={0} | all-to-all | bytes 524288 | tf_op jit(solution)/shard_map/all_to_all | solution.py:192
  111.8 1.1 broadcast_in_dim.31
  112.9 3.5 %all-to-all-start.9 = ((bf16[4,64,2048]{2,1,0:T(8,128)(2,1)}), bf16[4,64,2048]{2,1,0:T(8,128)(2,1)S(1)}, u32[]{:S(2)}, u32[]{:S(2)}) async-start(bf16[4,64,2048]{2,1,0:T(8,128)(2,1)} %broadcast_in_dim.31), calls=%async_computation.9 | async-start | bytes 2097152 | tf_op jit(solution)/shard_map/all_to_all | solution.py:192
  116.4 8.5 %shard_map.102 = bf16[256,640]{1,0:T(8,128)(2,1)S(1)} custom-call(bf16[256,512]{1,0:T(8,128)(2,1)S(1)} %bitcast.33, bf16[2048,256]{1,0:T(8,128)(2,1)} %bitcast.6.pairs), custom_call_target="tpu_custom_call" | custom-call | flops 5000000000 | bytes 1000000 | tf_op jit(solution)/shard_map/pallas_call | solution.py:230
  124.9 0.7 copy-done.4
  125.7 4.9 %all-to-all-done.9 = bf16[4,64,2048]{2,1,0:T(8,128)(2,1)S(1)} async-done(((bf16[4,64,2048]{2,1,0:T(8,128)(2,1)}), bf16[4,64,2048]{2,1,0:T(8,128)(2,1)S(1)}, u32[]{:S(2)}, u32[]{:S(2)}) %all-to-all-start.9) | async-done | bytes 1048608 | tf_op jit(solution)/shard_map/all_to_all | solution.py:192
  130.5 12.7 %all_to_all.52.arrived = bf16[8,32,640]{2,1,0:T(8,128)(2,1)S(1)} all-to-all(bf16[8,32,640]{2,1,0:T(8,128)(2,1)} %bitcast.32), channel_id=1, replica_groups=mesh['z'=8,'y'=8,'x'=4,'c'=2] {'x','c'}, dimensions={0} | all-to-all | bytes 655360 | tf_op jit(solution)/shard_map/all_to_all | solution.py:240
  143.2 1.1 broadcast_in_dim.30
  144.3 6.3 %all-to-all-start.7 = ((bf16[64,32,256]{2,1,0:T(8,128)(2,1)}), bf16[64,32,256]{2,1,0:T(8,128)(2,1)}, u32[]{:S(2)}, u32[]{:S(2)}) async-start(bf16[64,32,256]{2,1,0:T(8,128)(2,1)} %broadcast_in_dim.30), calls=%async_computation.7 | async-start | bytes 2097152 | tf_op jit(solution)/shard_map/all_to_all | solution.py:192
  150.6 2.9 %collective-permute-start.1 = (bf16[256,2048]{1,0:T(8,128)(2,1)S(1)}, bf16[256,2048]{1,0:T(8,128)(2,1)S(1)}, u32[]{:S(2)}, u32[]{:S(2)}) collective-permute-start(bf16[256,2048]{1,0:T(8,128)(2,1)S(1)} %bitcast.28), channel_id=1, source_target_pairs={{0,1},{1,0},{2,3},{3,2},{4,5},{5,4},{6,7},{7,6},{8,9},{9,8},{10,11... | collective-permute-start | bytes 3145736 | tf_op jit(solution)/shard_map/ppermute | solution.py:208
  153.5 1.9 collective-permute-start.2
  155.5 2.4 %collective-permute-start.3 = (bf16[256,2048]{1,0:T(8,128)(2,1)S(1)}, bf16[256,2048]{1,0:T(8,128)(2,1)}, u32[]{:S(2)}, u32[]{:S(2)}) collective-permute-start(bf16[256,2048]{1,0:T(8,128)(2,1)S(1)} %bitcast.26), channel_id=1, source_target_pairs={{0,1},{1,0},{2,3},{3,2},{4,5},{5,4},{6,7},{7,6},{8,9},{9,8},{10,11... | collective-permute-start | bytes 3145736 | tf_op jit(solution)/shard_map/ppermute | solution.py:208
  157.9 0.0 collective-permute-done.1.out_other
  157.9 0.2 collective-permute-done.2.other
  158.1 0.9 copy-done.3
  159.0 1.5 shard_map.103
  160.5 0.0 copy-start.6
  160.5 0.6 copy-done.6
  161.1 16.8 %all-to-all-done.7 = bf16[64,32,256]{2,1,0:T(8,128)(2,1)} async-done(((bf16[64,32,256]{2,1,0:T(8,128)(2,1)}), bf16[64,32,256]{2,1,0:T(8,128)(2,1)}, u32[]{:S(2)}, u32[]{:S(2)}) %all-to-all-start.7) | async-done | bytes 1048608 | tf_op jit(solution)/shard_map/all_to_all | solution.py:192
  177.9 12.2 %all_to_all.53 = bf16[8,32,512]{2,1,0:T(8,128)(2,1)S(1)} all-to-all(bf16[8,32,512]{2,1,0:T(8,128)(2,1)S(1)} %broadcast_in_dim.29), channel_id=1, replica_groups=mesh['z'=8,'y'=8,'x'=4,'c'=2] {'x','c'}, dimensions={0} | all-to-all | bytes 524288 | tf_op jit(solution)/shard_map/all_to_all | solution.py:192
  190.1 9.3 %shard_map.104 = bf16[256,640]{1,0:T(8,128)(2,1)} custom-call(bf16[256,512]{1,0:T(8,128)(2,1)S(1)} %bitcast.34, bf16[2048,256]{1,0:T(8,128)(2,1)} %bitcast.14.pairs), custom_call_target="tpu_custom_call" | custom-call | flops 5000000000 | bytes 1000000 | tf_op jit(solution)/shard_map/pallas_call | solution.py:230
  199.3 4.5 %all-to-all-start.8 = ((bf16[8,32,640]{2,1,0:T(8,128)(2,1)}), bf16[8,32,640]{2,1,0:T(8,128)(2,1)S(1)}, u32[]{:S(2)}, u32[]{:S(2)}) async-start(bf16[8,32,640]{2,1,0:T(8,128)(2,1)} %bitcast.15), calls=%async_computation.8 | async-start | bytes 655360 | tf_op jit(solution)/shard_map/all_to_all | solution.py:240
  203.8 0.0 collective-permute-done.3.out_other
  203.8 7.1 %all-to-all-done.8.arrived = bf16[8,32,640]{2,1,0:T(8,128)(2,1)S(1)} async-done(((bf16[8,32,640]{2,1,0:T(8,128)(2,1)}), bf16[8,32,640]{2,1,0:T(8,128)(2,1)S(1)}, u32[]{:S(2)}, u32[]{:S(2)}) %all-to-all-start.8) | async-done | bytes 327712 | tf_op jit(solution)/shard_map/all_to_all | solution.py:240
  210.9 2.5 %shard_map.105 = bf16[32,2048]{1,0:T(8,128)(2,1)} custom-call(s32[1]{0:T(128)} %bitcast.core_ref, bf16[8,32,640]{2,1,0:T(8,128)(2,1)S(1)} %all-to-all-done.8.arrived, bf16[32,2048]{1,0:T(8,128)(2,1)S(1)} %copy-done.7, bf16[256,2048]{1,0:T(8,128)(2,1)S(1)} %bitcast.27, bf16[256,2048]{1,0:T(8,128)(2,1)} %collective-permute-done.3.out_other), custom_call_target="tpu_custom_call" | custom-call | flops 200000000 | bytes 1000000 | tf_op jit(solution)/shard_map/pallas_call | solution.py:249
  (21 shorter events, 0.1 us)
Async XLA Ops:
  2.2 5.0 %copy-start.13 = (bf16[2,64,2048]{2,1,0:T(8,128)(2,1)S(1)}, bf16[2,64,2048]{2,1,0:T(8,128)(2,1)}, u32[]{:S(2)}) copy-start(bf16[2,64,2048]{2,1,0:T(8,128)(2,1)} %param.19) | copy-start | bytes 1572868
  2.2 14.7 %all-to-all-start = ((bf16[4,64,2048]{2,1,0:T(8,128)(2,1)}), bf16[4,64,2048]{2,1,0:T(8,128)(2,1)S(1)}, u32[]{:S(2)}, u32[]{:S(2)}) async-start(bf16[4,64,2048]{2,1,0:T(8,128)(2,1)} %broadcast_in_dim.24), calls=%async_computation | async-start | bytes 2097152 | tf_op jit(solution)/shard_map/all_to_all | solution.py:192
  30.3 3.7 %copy-start.5 = (bf16[32,2048]{1,0:T(8,128)(2,1)S(1)}, bf16[32,2048]{1,0:T(8,128)(2,1)}, u32[]{:S(2)}) copy-start(bf16[32,2048]{1,0:T(8,128)(2,1)} %source.1) | copy-start | bytes 393220
  30.3 3.7 %copy-start.9 = (f32[2,2048]{1,0:T(2,128)S(1)}, f32[2,2048]{1,0:T(2,128)}, u32[]{:S(2)}) copy-start(f32[2,2048]{1,0:T(2,128)} %gain.4) | copy-start | bytes 49156
  30.3 3.7 %copy-start.11 = (f32[2,64]{1,0:T(2,128)S(1)}, f32[2,64]{1,0:T(2,128)}, u32[]{:S(2)}) copy-start(f32[2,64]{1,0:T(2,128)} %key_gain.1) | copy-start | bytes 1540
  30.3 13.4 %all-to-all-start.5 = ((bf16[4,64,2048]{2,1,0:T(8,128)(2,1)}), bf16[4,64,2048]{2,1,0:T(8,128)(2,1)S(1)}, u32[]{:S(2)}, u32[]{:S(2)}) async-start(bf16[4,64,2048]{2,1,0:T(8,128)(2,1)} %broadcast_in_dim.28), calls=%async_computation.5 | async-start | bytes 2097152 | tf_op jit(solution)/shard_map/all_to_all | solution.py:192
  33.9 1.2 copy-start
  35.2 1.2 copy-start.1
  44.7 35.8 %copy-start.2 = (bf16[32,2048]{1,0:T(8,128)(2,1)S(1)}, bf16[32,2048]{1,0:T(8,128)(2,1)}, u32[]{:S(2)}) copy-start(bf16[32,2048]{1,0:T(8,128)(2,1)} %hidden.1) | copy-start | bytes 393220
  44.7 35.8 %copy-start.8 = (f32[2,2048]{1,0:T(2,128)S(1)}, f32[2,2048]{1,0:T(2,128)}, u32[]{:S(2)}) copy-start(f32[2,2048]{1,0:T(2,128)} %gain.5) | copy-start | bytes 49156
  44.7 52.5 %all-to-all-start.2 = ((bf16[64,32,256]{2,1,0:T(8,128)(2,1)}), bf16[64,32,256]{2,1,0:T(8,128)(2,1)}, u32[]{:S(2)}, u32[]{:S(2)}) async-start(bf16[64,32,256]{2,1,0:T(8,128)(2,1)} %broadcast_in_dim.26), calls=%async_computation.2 | async-start | bytes 2097152 | tf_op jit(solution)/shard_map/all_to_all | solution.py:192
  72.1 8.4 %collective-permute-start = (bf16[256,2048]{1,0:T(8,128)(2,1)S(1)}, bf16[256,2048]{1,0:T(8,128)(2,1)}, u32[]{:S(2)}, u32[]{:S(2)}) collective-permute-start(bf16[256,2048]{1,0:T(8,128)(2,1)S(1)} %bitcast.24), channel_id=1, source_target_pairs={{0,1},{1,0},{2,3},{3,2},{4,5},{5,4},{6,7},{7,6},{8,9},{9,8},{10,11... | collective-permute-start | bytes 3145736 | tf_op jit(solution)/shard_map/ppermute | solution.py:208
  78.1 2.4 %copy-start.10 = (f32[2,64]{1,0:T(2,128)S(1)}, f32[2,64]{1,0:T(2,128)}, u32[]{:S(2)}) copy-start(f32[2,64]{1,0:T(2,128)} %query_gain.3) | copy-start | bytes 1540
  97.3 14.5 %copy-start.12 = (bf16[64,2048]{1,0:T(8,128)(2,1)S(1)}, bf16[64,2048]{1,0:T(8,128)(2,1)}, u32[]{:S(2)}) copy-start(bf16[64,2048]{1,0:T(8,128)(2,1)} %get-tuple-element.9) | copy-start | bytes 786436
  112.9 17.6 %all-to-all-start.9 = ((bf16[4,64,2048]{2,1,0:T(8,128)(2,1)}), bf16[4,64,2048]{2,1,0:T(8,128)(2,1)S(1)}, u32[]{:S(2)}, u32[]{:S(2)}) async-start(bf16[4,64,2048]{2,1,0:T(8,128)(2,1)} %broadcast_in_dim.31), calls=%async_computation.9 | async-start | bytes 2097152 | tf_op jit(solution)/shard_map/all_to_all | solution.py:192
  124.9 0.7 copy-start.4
  144.3 33.5 %all-to-all-start.7 = ((bf16[64,32,256]{2,1,0:T(8,128)(2,1)}), bf16[64,32,256]{2,1,0:T(8,128)(2,1)}, u32[]{:S(2)}, u32[]{:S(2)}) async-start(bf16[64,32,256]{2,1,0:T(8,128)(2,1)} %broadcast_in_dim.30), calls=%async_computation.7 | async-start | bytes 2097152 | tf_op jit(solution)/shard_map/all_to_all | solution.py:192
  150.6 7.3 %collective-permute-start.1 = (bf16[256,2048]{1,0:T(8,128)(2,1)S(1)}, bf16[256,2048]{1,0:T(8,128)(2,1)S(1)}, u32[]{:S(2)}, u32[]{:S(2)}) collective-permute-start(bf16[256,2048]{1,0:T(8,128)(2,1)S(1)} %bitcast.28), channel_id=1, source_target_pairs={{0,1},{1,0},{2,3},{3,2},{4,5},{5,4},{6,7},{7,6},{8,9},{9,8},{10,11... | collective-permute-start | bytes 3145736 | tf_op jit(solution)/shard_map/ppermute | solution.py:208
  153.5 4.6 %collective-permute-start.2 = (bf16[256,2048]{1,0:T(8,128)(2,1)S(1)}, bf16[256,2048]{1,0:T(8,128)(2,1)S(1)}, u32[]{:S(2)}, u32[]{:S(2)}) collective-permute-start(bf16[256,2048]{1,0:T(8,128)(2,1)S(1)} %bitcast.30), channel_id=1, source_target_pairs={{0,1},{1,0},{2,3},{3,2},{4,5},{5,4},{6,7},{7,6},{8,9},{9,8},{10,11... | collective-permute-start | bytes 3145736 | tf_op jit(solution)/shard_map/ppermute | solution.py:208
  155.5 48.4 %collective-permute-start.3 = (bf16[256,2048]{1,0:T(8,128)(2,1)S(1)}, bf16[256,2048]{1,0:T(8,128)(2,1)}, u32[]{:S(2)}, u32[]{:S(2)}) collective-permute-start(bf16[256,2048]{1,0:T(8,128)(2,1)S(1)} %bitcast.26), channel_id=1, source_target_pairs={{0,1},{1,0},{2,3},{3,2},{4,5},{5,4},{6,7},{7,6},{8,9},{9,8},{10,11... | collective-permute-start | bytes 3145736 | tf_op jit(solution)/shard_map/ppermute | solution.py:208
  158.1 0.9 copy-start.3
  160.5 0.7 copy-start.6
  199.3 11.6 %copy-start.7 = (bf16[32,2048]{1,0:T(8,128)(2,1)S(1)}, bf16[32,2048]{1,0:T(8,128)(2,1)}, u32[]{:S(2)}) copy-start(bf16[32,2048]{1,0:T(8,128)(2,1)} %copy-done.6) | copy-start | bytes 393220
  199.3 11.6 %all-to-all-start.8 = ((bf16[8,32,640]{2,1,0:T(8,128)(2,1)}), bf16[8,32,640]{2,1,0:T(8,128)(2,1)S(1)}, u32[]{:S(2)}, u32[]{:S(2)}) async-start(bf16[8,32,640]{2,1,0:T(8,128)(2,1)} %bitcast.15), calls=%async_computation.8 | async-start | bytes 655360 | tf_op jit(solution)/shard_map/all_to_all | solution.py:240

commit v2 on v1

v2 whole, which is shorter than its diff:
```python
import functools

import jax
import jax.numpy as jnp
from jax import lax
from jax.experimental import pallas as pl
from jax.experimental.pallas import tpu as pltpu
from jax.sharding import Mesh
from jax.sharding import PartitionSpec as P

ROWS = ("z", "y")
TP = ("x", "c")
ALL = ("z", "y", "x", "c")
EPS = 1e-06
LOG2E = 1.4426950408889634
F32 = jnp.float32
BF16 = jnp.bfloat16


def dot(a, b):
    return jnp.dot(a, b, preferred_element_type=F32)


def dot_t(a, b):
    return lax.dot_general(a, b, (((1,), (1,)), ((), ())), preferred_element_type=F32)


def rms(value):
    return lax.rsqrt(jnp.mean(value * value, axis=-1, keepdims=True) + EPS)


def head_norm(value, gain_row, head):
    rows, width = value.shape
    low = lax.broadcasted_iota(jnp.int32, (rows, 2 * head), 1) < head
    groups = []
    for start in range(0, width, 2 * head):
        part = value[:, start : start + 2 * head]
        square = part * part
        first = jnp.sum(jnp.where(low, square, 0.0), axis=-1, keepdims=True)
        second = jnp.sum(jnp.where(low, 0.0, square), axis=-1, keepdims=True)
        scale = lax.rsqrt(jnp.where(low, first, second) / head + EPS)
        groups.append(part * scale * gain_row)
    return groups


def doubled(row):
    return jnp.concatenate([row, row], axis=-1)


def source_kernel(source, gain, key_gain, key_weight, value_weight, out):
    layers, head = key_gain.shape
    value = source[...].astype(F32)
    scaled = value * rms(value)
    width = key_weight.shape[2]
    for layer in range(layers):
        normed = (scaled * gain[layer : layer + 1, :]).astype(BF16)
        keys = dot(normed, key_weight[layer])
        row = doubled(key_gain[layer : layer + 1, :])
        groups = head_norm(keys, row, head)
        for k, group in enumerate(groups):
            out[layer, :, k * 2 * head : (k + 1) * 2 * head] = group.astype(BF16)
        out[layer, :, width:] = dot(normed, value_weight[layer]).astype(BF16)


def store_groups(out, groups):
    width = groups[0].shape[1]
    for k, group in enumerate(groups):
        out[:, k * width : (k + 1) * width] = group.astype(BF16)


def project(value, gain_row, weight, query_gain, layer, out):
    head = query_gain.shape[1]
    normed = (value * rms(value) * gain_row).astype(BF16)
    row = doubled(query_gain[layer : layer + 1, :])
    store_groups(out, head_norm(dot_t(normed, weight[...]), row, head))


def query_kernel(layer, target, gain, query_gain, weight, out):
    project(target[...].astype(F32), gain[layer : layer + 1, :], weight, query_gain, layer, out)


def mixed(arrived, hidden, weight, heads, head):
    total = arrived[0].astype(F32)
    for k in range(1, arrived.shape[0]):
        total = total + arrived[k].astype(F32)
    rows = total.shape[0]
    width = heads * head
    mass = total[:, width : width + heads] + total[:, width + heads : width + 2 * heads]
    low = lax.broadcasted_iota(jnp.int32, (rows, 2 * head), 1) < head
    branch = None
    for g in range(heads // 2):
        below = jnp.where(low, mass[:, 2 * g : 2 * g + 1], mass[:, 2 * g + 1 : 2 * g + 2])
        columns = slice(2 * g * head, 2 * (g + 1) * head)
        part = dot((total[:, columns] / below).astype(BF16), weight[columns, :])
        branch = part if branch is None else branch + part
    return (hidden[...].astype(F32) + branch).astype(BF16)


def middle_kernel(layer, heads, arrived, hidden, gain, query_gain, out_weight, weight, hidden_out, out):
    now = mixed(arrived, hidden, out_weight, heads, query_gain.shape[1])
    hidden_out[...] = now
    project(now.astype(F32), gain[layer : layer + 1, :], weight, query_gain, layer, out)


def last_kernel(heads, head, arrived, hidden, out_weight, hidden_out):
    hidden_out[...] = mixed(arrived, hidden, out_weight, heads, head)


def attention_kernel(heads, head, tile, queries, pairs, out, rhs, value_t, gathered):
    keys = pairs.shape[0]
    width = 2 * head
    columns = queries.shape[0]
    factor = LOG2E * head**-0.5
    turned = jnp.transpose(queries[...].astype(F32)).astype(BF16)
    zero = jnp.zeros((head, columns), BF16)
    per = heads // 2
    for p in range(heads):
        kv = p // per
        rhs[p, kv * head : (kv + 1) * head, :] = turned[p * head : (p + 1) * head, :]
        rhs[p, (1 - kv) * head : (2 - kv) * head, :] = zero
    value_t[...] = jnp.transpose(pairs[:, width:].astype(F32)).astype(BF16)
    for kv in range(2):

        def one_head(j, carry, kv=kv):
            p = kv * per + j
            right = rhs[p]
            mass = jnp.zeros((8, columns), F32)
            total = None
            for t in range(keys // tile):
                score = dot(pairs[t * tile : (t + 1) * tile, :width], right)
                weight = jnp.exp2(score * factor)
                mass = mass + jnp.sum(weight.reshape(tile // 8, 8, columns), axis=0)
                part = dot(value_t[:, t * tile : (t + 1) * tile], weight.astype(BF16))
                total = part if total is None else total + part
            gathered[pl.ds(pl.multiple_of(p * head, head), head), :] = total[kv * head : (kv + 1) * head, :]
            mass = jnp.sum(mass, axis=0, keepdims=True)
            top = mass.astype(BF16).astype(F32)
            gathered[pl.ds(heads * head + p, 1), :] = top
            gathered[pl.ds(heads * head + heads + p, 1), :] = mass - top
            return carry

        lax.fori_loop(0, per, one_head, 0)
    rest = heads * head + 2 * heads
    gathered[rest:, :] = jnp.zeros((gathered.shape[0] - rest, columns), F32)
    out[...] = jnp.transpose(gathered[...]).astype(BF16)


def call(kernel, shapes, scratch=(), flops=1000000):
    one = not isinstance(shapes, (list, tuple))
    specs = pl.BlockSpec(memory_space=pltpu.VMEM)
    return pl.pallas_call(
        kernel,
        out_shape=shapes,
        out_specs=specs if one else [specs] * len(shapes),
        scratch_shapes=list(scratch),
        compiler_params=pltpu.CompilerParams(vmem_limit_bytes=40 * 1024 * 1024),
        cost_estimate=pl.CostEstimate(flops=flops, bytes_accessed=1000000, transcendentals=0),
    )


def to_all(value, axis):
    copies = jnp.broadcast_to(value, (lax.axis_size(axis), *value.shape))
    return lax.all_to_all(copies, axis, split_axis=0, concat_axis=0, tiled=True)


def body(target, source, target_gain, source_gain, query_gain, key_gain, query_weight, key_weight, value_weight, out_weight):
    layers, _, head_columns = query_weight.shape
    head = query_gain.shape[1]
    heads = head_columns // head * lax.axis_size(TP)
    rows, model = target.shape
    group = rows * lax.axis_size(TP)
    shapes = jax.ShapeDtypeStruct
    query_t = jnp.swapaxes(query_weight, 1, 2)
    width = heads * head
    wide = width + 128

    with jax.named_scope("keys"):
        pairs = call(source_kernel, shapes((layers, rows, 4 * head), BF16), flops=200000000)(
            source, source_gain, key_gain, key_weight, value_weight
        )
        plane = to_all(pairs, "z")
        columns = [plane[:, layer].reshape(-1, 4 * head) for layer in range(layers)]

    def full(piece, name):
        with jax.named_scope(name):
            return lax.all_gather(piece, TP, tiled=True)

    def line(piece, name):
        with jax.named_scope(name):
            return lax.all_gather(piece, "y", tiled=True)

    query_full = [full(query_t[0], "wq0")]
    arrived_pairs = [line(columns[0], "kv0")]
    out_full = [full(out_weight[0], "wo0")]
    query_full.append(full(query_t[1], "wq1"))
    arrived_pairs.append(line(columns[1], "kv1"))
    out_full.append(full(out_weight[1], "wo1"))

    queries = call(functools.partial(query_kernel, 0), shapes((rows, width), BF16), flops=200000000)(
        target, target_gain, query_gain, query_full[0]
    )
    hidden = target
    for layer in range(layers):
        everyone = to_all(queries, TP).reshape(group, width)
        kv = arrived_pairs[layer]
        partial = call(
            functools.partial(attention_kernel, heads, head, 256),
            shapes((group, wide), BF16),
            scratch=[
                pltpu.VMEM((heads, 2 * head, group), BF16),
                pltpu.VMEM((2 * head, kv.shape[0]), BF16),
                pltpu.VMEM((wide, group), F32),
            ],
            flops=5000000000,
        )(everyone, kv)
        arrived = lax.all_to_all(partial.reshape(-1, rows, wide), TP, split_axis=0, concat_axis=0, tiled=True)
        if layer + 1 < layers:
            hidden, queries = call(
                functools.partial(middle_kernel, layer + 1, heads),
                [shapes((rows, model), BF16), shapes((rows, width), BF16)],
                flops=400000000,
            )(arrived, hidden, target_gain, query_gain, out_full[layer], query_full[layer + 1])
        else:
            hidden = call(functools.partial(last_kernel, heads, head), shapes((rows, model), BF16), flops=200000000)(
                arrived, hidden, out_full[layer]
            )
    return hidden


def solution(mesh):
    columns = mesh.shape["tp"]
    split = Mesh(mesh.devices.reshape(8, 8, columns // 2, 2), ALL)
    return jax.shard_map(
        body,
        mesh=split,
        in_specs=(P(ALL, None), P(ALL, None), P(), P(), P(), P(), P(None, None, TP), P(), P(), P(None, TP, None)),
        out_specs=P(ALL, None),
        check_vma=False,
    )
```

time: 215 us -> 241 us (1.12)
  waiting for transfers between devices: 61.7 us -> 140 us
  starting transfers between devices: 63.5 us -> 27 us
  blocking collectives: 51.5 us -> 21.3 us
  between operations: 0.23 us -> 13.6 us
  local copies, waits for them, and re-layouts: 12.2 us -> 18.5 us
  Pallas kernels: 24.3 us -> 19.9 us
    all_gather x0 -> x6, waiting for transfers between devices: none -> 138 us  [the longest x4 77.9 us: full(): return lax.all_gather(piece, TP, tiled=True)]
    all_to_all x5 -> x2, waiting for transfers between devices: 52 us -> 0.01 us  [to_all(): return lax.all_to_all(copies, axis, split_axis=0, concat_axis=0, tiled=True)]
    all_to_all x5 -> x2, starting transfers between devices: 45.7 us -> 7.34 us  [to_all(): return lax.all_to_all(copies, axis, split_axis=0, concat_axis=0, tiled=True)]
    all_to_all x3 -> x1, blocking collectives: 38.8 us -> 21.3 us  [to_all(): return lax.all_to_all(copies, axis, split_axis=0, concat_axis=0, tiled=True)]
    all_to_all x1 -> x2, starting transfers between devices: 4.51 us -> 19.5 us  [body(): lax.all_to_all(partial.reshape(-1, rows, wide), TP, split_axis=0, concat_...]
    ppermute x4 -> x0, starting transfers between devices: 13.3 us -> none  [full(): other = lax.ppermute(mine, 'c', [(0, 1), (1, 0)])]
    all_to_all x1 -> x0, blocking collectives: 12.7 us -> none  [body(): lax.all_to_all(partial.reshape(-1, rows, wide), TP, split_axis=0, concat_...]
    unnamed x28 -> x30, local copies, waits for them, and re-layouts: 4.75 us -> 13.6 us
  transfers between devices with their start and end apart: 10 -> 10, of which waited for: 8 -> 6; matrix products, arithmetic and copies ran while one was open for 0% -> 1% of each run, Pallas kernels for 10% -> 8%
where the time goes in v2:
time: 241 us; the launch traced here: 240 us
  waiting for transfers between devices  140 us (58%)
  starting transfers between devices  27 us (11%)
  blocking collectives  21.3 us (9%)
  Pallas kernels  19.9 us (8%)
  local copies, waits for them, and re-layouts  18.5 us (8%)
  between operations  13.6 us (6%)
    all_gather x4, waiting for transfers between devices, full(): return lax.all_gather(piece, TP, tiled=True)  77.9 us
    all_gather x2, waiting for transfers between devices, line(): return lax.all_gather(piece, 'y', tiled=True)  60.2 us
    all_to_all x1, blocking collectives, to_all(): return lax.all_to_all(copies, axis, split_axis=0, concat_axis=0, tiled=True)  21.3 us
    all_to_all x2, starting transfers between devices, body(): lax.all_to_all(partial.reshape(-1, rows, wide), TP, split_axis=0, concat_...  19.5 us
    pallas_call x2, Pallas kernels, body(): call(functools.partial(attention_kernel, heads, head, 256), shapes((group...  15.9 us
    unnamed x30, local copies, waits for them, and re-layouts  13.6 us
    all_to_all x2, starting transfers between devices, to_all(): return lax.all_to_all(copies, axis, split_axis=0, concat_axis=0, tiled=True)  7.34 us
  transfers between devices with their start and end apart: 10, of which 6 were waited for; matrix products, arithmetic and copies ran while one was open for 1% of the time, Pallas kernels for 8%

profile of v2, /device:TPU:1, one launch (start us, length us, event | category | flops | bytes accessed | tf_op | source)
XLA Modules:
  0.0 240.0 jit_solution(4445442405256078079)
XLA Ops:
  6.5 1.9 fusion.1
  8.5 0.0 all-gather.15.cloned.1.call-update
  8.5 0.0 all-gather.11.cloned.1.call-start
  8.5 0.0 copy-start.4
  8.6 1.2 copy-done.4
  9.8 1.2 copy-done.5
  11.0 0.9 copy-done.7
  11.9 0.7 copy-done.9
  12.6 0.7 copy-done.11
  13.3 0.5 keys.1
  13.8 0.0 copy-start.6
  13.8 0.0 copy-start.8
  13.9 0.0 copy-start.10
  13.9 21.3 %all_to_all.25 = bf16[8,2,32,256]{3,2,1,0:T(8,128)(2,1)S(1)} all-to-all(bf16[8,2,32,256]{3,2,1,0:T(8,128)(2,1)S(1)} %broadcast_in_dim.10), channel_id=1, replica_groups=mesh['z'=8,'y'=8,'x'=4,'c'=2] {'z'}, dimensions={0} | all-to-all | bytes 524288 | tf_op jit(solution)/shard_map/keys/all_to_all | solution.py:163
  35.2 0.7 fusion.2
  35.9 0.0 all-gather.11.cloned.1.call-update
  35.9 0.0 all-gather.17.cloned.1.call-start
  36.0 0.8 fusion
  36.8 0.0 all-gather.17.cloned.1.call-update
  36.8 0.0 all-gather.19.cloned.1.call-start
  36.9 0.5 all-gather.19.cloned.1.call-update
  37.4 0.0 all-gather.13.cloned.1.call-start
  37.5 0.5 all-gather.13.cloned.1.call-update
  38.0 0.0 all-gather.21.cloned.1.call-start
  38.1 0.5 all-gather.21.cloned.1.call-update
  38.6 7.4 %all-gather.15.cloned.1.call-done = bf16[1,512,2048]{2,1,0:T(8,128)(2,1)} async-done(((bf16[1,64,2048]{2,1,0:T(8,128)(2,1)}), bf16[1,512,2048]{2,1,0:T(8,128)(2,1)}) %all-gather.15.cloned.1.call-update) | async-done | bytes 2097168 | tf_op jit(solution)/shard_map/wq0/all_gather | solution.py:186
  46.0 1.6 copy-done.3
  47.6 0.9 shard_map.100
  48.5 0.7 broadcast_in_dim.9
  49.2 3.7 %all-to-all-start = ((bf16[8,32,512]{2,1,0:T(8,128)(2,1)}), bf16[8,32,512]{2,1,0:T(8,128)(2,1)S(1)}, u32[]{:S(2)}, u32[]{:S(2)}) async-start(bf16[8,32,512]{2,1,0:T(8,128)(2,1)} %broadcast_in_dim.9), calls=%async_computation | async-start | bytes 524288 | tf_op jit(solution)/shard_map/all_to_all | solution.py:163
  52.9 31.2 %all-gather.11.cloned.1.call-done.pairs = bf16[2048,256]{1,0:T(8,128)(2,1)} async-done(((bf16[256,256]{1,0:T(8,128)(2,1)}), bf16[2048,256]{1,0:T(8,128)(2,1)}) %all-gather.11.cloned.1.call-update) | async-done | bytes 1048592 | tf_op jit(solution)/shard_map/kv0/all_gather | solution.py:190
  84.1 1.2 copy-done.13
  85.3 7.9 %shard_map.101 = bf16[256,640]{1,0:T(8,128)(2,1)} custom-call(bf16[256,512]{1,0:T(8,128)(2,1)S(1)} %bitcast.15, bf16[2048,256]{1,0:T(8,128)(2,1)S(1)} %copy-done.13), custom_call_target="tpu_custom_call" | custom-call | flops 5000000000 | bytes 1000000 | tf_op jit(solution)/shard_map/pallas_call | solution.py:206
  93.3 9.7 %all-to-all-start.2 = ((bf16[8,32,640]{2,1,0:T(8,128)(2,1)}), bf16[8,32,640]{2,1,0:T(8,128)(2,1)S(1)}, u32[]{:S(2)}, u32[]{:S(2)}) async-start(bf16[8,32,640]{2,1,0:T(8,128)(2,1)} %bitcast.4), calls=%async_computation.2 | async-start | bytes 655360 | tf_op jit(solution)/shard_map/all_to_all | solution.py:216
  103.0 19.2 %all-gather.17.cloned.1.call-done = bf16[1,512,2048]{2,1,0:T(8,128)(2,1)} async-done(((bf16[1,64,2048]{2,1,0:T(8,128)(2,1)}), bf16[1,512,2048]{2,1,0:T(8,128)(2,1)}) %all-gather.17.cloned.1.call-update) | async-done | bytes 2097168 | tf_op jit(solution)/shard_map/wo0/all_gather | solution.py:186
  122.3 32.0 %all-gather.19.cloned.1.call-done = bf16[1,512,2048]{2,1,0:T(8,128)(2,1)} async-done(((bf16[1,64,2048]{2,1,0:T(8,128)(2,1)}), bf16[1,512,2048]{2,1,0:T(8,128)(2,1)}) %all-gather.19.cloned.1.call-update) | async-done | bytes 2097168 | tf_op jit(solution)/shard_map/wq1/all_gather | solution.py:186
  154.2 1.6 copy-done
  155.8 1.6 copy-done.1
  157.4 1.4 shard_map.102
  158.8 0.7 broadcast_in_dim.11
  159.5 3.7 %all-to-all-start.3 = ((bf16[8,32,512]{2,1,0:T(8,128)(2,1)}), bf16[8,32,512]{2,1,0:T(8,128)(2,1)S(1)}, u32[]{:S(2)}, u32[]{:S(2)}) async-start(bf16[8,32,512]{2,1,0:T(8,128)(2,1)} %broadcast_in_dim.11), calls=%async_computation.3 | async-start | bytes 524288 | tf_op jit(solution)/shard_map/all_to_all | solution.py:163
  163.2 29.0 %all-gather.13.cloned.1.call-done.pairs = bf16[2048,256]{1,0:T(8,128)(2,1)} async-done(((bf16[256,256]{1,0:T(8,128)(2,1)}), bf16[2048,256]{1,0:T(8,128)(2,1)}) %all-gather.13.cloned.1.call-update) | async-done | bytes 1048592 | tf_op jit(solution)/shard_map/kv1/all_gather | solution.py:190
  192.2 1.2 copy-done.12
  193.4 7.9 %shard_map.103 = bf16[256,640]{1,0:T(8,128)(2,1)} custom-call(bf16[256,512]{1,0:T(8,128)(2,1)S(1)} %bitcast.16, bf16[2048,256]{1,0:T(8,128)(2,1)S(1)} %copy-done.12), custom_call_target="tpu_custom_call" | custom-call | flops 5000000000 | bytes 1000000 | tf_op jit(solution)/shard_map/pallas_call | solution.py:206
  201.4 9.8 %all-to-all-start.4 = ((bf16[8,32,640]{2,1,0:T(8,128)(2,1)}), bf16[8,32,640]{2,1,0:T(8,128)(2,1)S(1)}, u32[]{:S(2)}, u32[]{:S(2)}) async-start(bf16[8,32,640]{2,1,0:T(8,128)(2,1)} %bitcast.9), calls=%async_computation.4 | async-start | bytes 655360 | tf_op jit(solution)/shard_map/all_to_all | solution.py:216
  211.1 19.2 %all-gather.21.cloned.1.call-done = bf16[1,512,2048]{2,1,0:T(8,128)(2,1)} async-done(((bf16[1,64,2048]{2,1,0:T(8,128)(2,1)}), bf16[1,512,2048]{2,1,0:T(8,128)(2,1)}) %all-gather.21.cloned.1.call-update) | async-done | bytes 2097168 | tf_op jit(solution)/shard_map/wo1/all_gather | solution.py:186
  230.4 1.6 copy-done.2
  232.0 1.2 shard_map.104
  (21 shorter events, 0.1 us)
Async XLA Ops:
  6.5 39.5 %all-gather.15.cloned.1.call-start = ((), (), s32[]{:S(2)}) async-start(), calls=%async_computation.7 | async-start | bytes 2359296 | tf_op jit(solution)/shard_map/wq0/all_gather | solution.py:186
  6.5 29.4 %copy-start.14 = (bf16[2,64,2048]{2,1,0:T(8,128)(2,1)S(1)}, bf16[2,64,2048]{2,1,0:T(8,128)(2,1)}, u32[]{:S(2)}) copy-start(bf16[2,64,2048]{2,1,0:T(8,128)(2,1)} %param.19) | copy-start | bytes 1572868
  8.5 75.6 %all-gather.11.cloned.1.call-start = ((), (), s32[]{:S(2)}) async-start(), calls=%async_computation.5 | async-start | bytes 1179648 | tf_op jit(solution)/shard_map/kv0/all_gather | solution.py:190
  8.5 1.2 copy-start.4
  9.8 1.2 copy-start.5
  11.0 0.9 copy-start.7
  11.9 0.7 copy-start.9
  12.6 0.7 copy-start.11
  13.8 32.2 %copy-start.6 = (bf16[32,2048]{1,0:T(8,128)(2,1)S(1)}, bf16[32,2048]{1,0:T(8,128)(2,1)}, u32[]{:S(2)}) copy-start(bf16[32,2048]{1,0:T(8,128)(2,1)} %hidden.1) | copy-start | bytes 393220
  13.8 32.2 %copy-start.8 = (f32[2,2048]{1,0:T(2,128)S(1)}, f32[2,2048]{1,0:T(2,128)}, u32[]{:S(2)}) copy-start(f32[2,2048]{1,0:T(2,128)} %gain.5) | copy-start | bytes 49156
  13.9 32.2 %copy-start.10 = (f32[2,64]{1,0:T(2,128)S(1)}, f32[2,64]{1,0:T(2,128)}, u32[]{:S(2)}) copy-start(f32[2,64]{1,0:T(2,128)} %query_gain.3) | copy-start | bytes 1540
  35.9 86.3 %all-gather.17.cloned.1.call-start = ((), (), s32[]{:S(2)}) async-start(), calls=%async_computation.8 | async-start | bytes 2359296 | tf_op jit(solution)/shard_map/wo0/all_gather | solution.py:186
  36.8 117.4 %all-gather.19.cloned.1.call-start = ((), (), s32[]{:S(2)}) async-start(), calls=%async_computation.9 | async-start | bytes 2359296 | tf_op jit(solution)/shard_map/wq1/all_gather | solution.py:186
  37.4 154.8 %all-gather.13.cloned.1.call-start = ((), (), s32[]{:S(2)}) async-start(), calls=%async_computation.6 | async-start | bytes 1179648 | tf_op jit(solution)/shard_map/kv1/all_gather | solution.py:190
  38.0 192.3 %all-gather.21.cloned.1.call-start = ((), (), s32[]{:S(2)}) async-start(), calls=%async_computation.10 | async-start | bytes 2359296 | tf_op jit(solution)/shard_map/wo1/all_gather | solution.py:186
  46.0 1.6 copy-start.3
  49.2 34.9 %all-to-all-start = ((bf16[8,32,512]{2,1,0:T(8,128)(2,1)}), bf16[8,32,512]{2,1,0:T(8,128)(2,1)S(1)}, u32[]{:S(2)}, u32[]{:S(2)}) async-start(bf16[8,32,512]{2,1,0:T(8,128)(2,1)} %broadcast_in_dim.9), calls=%async_computation | async-start | bytes 524288 | tf_op jit(solution)/shard_map/all_to_all | solution.py:163
  84.1 1.2 copy-start.13
  93.3 61.0 %all-to-all-start.2 = ((bf16[8,32,640]{2,1,0:T(8,128)(2,1)}), bf16[8,32,640]{2,1,0:T(8,128)(2,1)S(1)}, u32[]{:S(2)}, u32[]{:S(2)}) async-start(bf16[8,32,640]{2,1,0:T(8,128)(2,1)} %bitcast.4), calls=%async_computation.2 | async-start | bytes 655360 | tf_op jit(solution)/shard_map/all_to_all | solution.py:216
  154.2 1.6 copy-start
  155.8 1.6 copy-start.1
  159.5 32.6 %all-to-all-start.3 = ((bf16[8,32,512]{2,1,0:T(8,128)(2,1)}), bf16[8,32,512]{2,1,0:T(8,128)(2,1)S(1)}, u32[]{:S(2)}, u32[]{:S(2)}) async-start(bf16[8,32,512]{2,1,0:T(8,128)(2,1)} %broadcast_in_dim.11), calls=%async_computation.3 | async-start | bytes 524288 | tf_op jit(solution)/shard_map/all_to_all | solution.py:163
  192.2 1.2 copy-start.12
  201.4 29.0 %all-to-all-start.4 = ((bf16[8,32,640]{2,1,0:T(8,128)(2,1)}), bf16[8,32,640]{2,1,0:T(8,128)(2,1)S(1)}, u32[]{:S(2)}, u32[]{:S(2)}) async-start(bf16[8,32,640]{2,1,0:T(8,128)(2,1)} %bitcast.9), calls=%async_computation.4 | async-start | bytes 655360 | tf_op jit(solution)/shard_map/all_to_all | solution.py:216
  230.4 1.6 copy-start.2
Sparse Core Ops, SparseCore 0:
  9.5 36.4 all-gather.14
  48.1 35.9 all-gather.10
  86.3 35.9 all-gather.16
  124.3 29.9 all-gather.18
  156.2 35.9 all-gather.12
  194.2 36.1 all-gather.20
